TPU v7x, 32 devices: a whole 2x2x4 slice. The times are simulated.
32 devices in a mesh: sp: 8 (over z, y), tp: 4 (over x, core).
Axes of the slice: x: 2, y: 2, z: 4, core: 2. Of those that a mesh axis runs over, the one named last changes fastest.
Arguments:
- tokens: bfloat16 [8192, 2048], P('sp'), may hold values from -6 to 6
- in_gain: float32 [2048], replicated, may hold values from 0.1 to 1.9
- w_query: bfloat16 [2048, 1024], P(None, 'tp'), may hold values from -0.125 to 0.125
- w_forget: bfloat16 [2048, 1024], P(None, 'tp'), may hold values from -0.125 to 0.125
- w_input: bfloat16 [2048, 1024], P(None, 'tp'), may hold values from -0.125 to 0.125
- w_outgate: bfloat16 [2048, 1024], P(None, 'tp'), may hold values from -0.125 to 0.125
- w_conv_h: bfloat16 [2048, 1024], P(None, 'tp'), may hold values from -0.125 to 0.125
- w_conv_b: bfloat16 [2048, 1024], P(None, 'tp'), may hold values from -0.125 to 0.125
- w_conv_c: bfloat16 [2048, 1024], P(None, 'tp'), may hold values from -0.125 to 0.125
- forget_floor: float32 [1024], P('tp'), may hold values from 0.84 to 1
- forget_leak: float32 [8192, 1024], P('sp', 'tp'), may hold values from -1 to 0
- state_gain: float32 [128], replicated, may hold values from 0.1 to 1.9
- conv_taps: bfloat16 [3, 1024], P(None, 'tp'), may hold values from -3.5 to 3.5
- group_gain: float32 [128], replicated, may hold values from 0.1 to 1.9
- out_state: bfloat16 [1024, 2048], P('tp'), may hold values from -0.1875 to 0.1875
- out_conv: bfloat16 [1024, 2048], P('tp'), may hold values from -0.1875 to 0.1875
Outputs:
- mixed_out: bfloat16 [8192, 2048], P('sp', 'tp')
All inputs are finite; a program needn't handle non-finite values.
Results may differ from a plain program's by a relative error of at most 0.015.
Values may be sent and summed in bfloat16 or wider, within the bound.
A program may use at most 128 MiB of HBM per device.

v0:
```python
import jax
import jax.numpy as jnp
from jax import lax
from jax.sharding import PartitionSpec as P

GROUP_FEATURES = 128
BLOCK = 64
TAPS = 3


norm_eps = 1e-06
highest = lax.Precision.HIGHEST


def from_behind(array, axis, by):
    count = lax.axis_size(axis)
    pairs = [(i, i + by) for i in range(count) if 0 <= i + by < count]
    return lax.ppermute(array, axis, pairs)


def carried_in(array, axis, join, neutral):
    place = lax.axis_index(axis)
    gathered = jax.tree.map(
        lambda a, kind: lax.all_gather(a.astype(kind), axis), array, (jnp.bfloat16, jnp.bfloat16)
    )
    state = jax.tree.map(lambda a, e: jnp.zeros_like(a) + jnp.asarray(e, a.dtype), array, neutral)

    def one(hop, state):
        return join(
            state,
            jax.tree.map(
                lambda a, own: lax.dynamic_index_in_dim(a, hop, 0, False).astype(own.dtype),
                gathered,
                array,
            ),
        )

    return lax.fori_loop(0, place, one, state)


def rms_rows(values, gain):
    scale = lax.rsqrt(jnp.mean(values * values, axis=-1, keepdims=True) + norm_eps)
    return values * scale * gain


def state_block(carry, inputs):
    carry_state, offset = carry
    query_blk, key_blk, value_blk, logf_blk = inputs
    cum_log = jnp.cumsum(logf_blk, axis=1)
    carried = jnp.einsum(
        "hcd,hde->hce", query_blk * jnp.exp(cum_log), carry_state, precision=highest
    )
    length = logf_blk.shape[1]
    causal = (jnp.arange(length)[:, None] >= jnp.arange(length)[None, :])[None, :, :, None]
    diff_log = cum_log[:, :, None, :] - cum_log[:, None, :, :]
    decay_all = jnp.exp(jnp.where(causal, diff_log, -jnp.inf))
    scores = jnp.einsum("hid,hjd,hijd->hij", query_blk, key_blk, decay_all, precision=highest)
    result = carried + jnp.einsum("hij,hje->hie", scores, value_blk, precision=highest)
    last_log = cum_log[:, -1, :]
    fresh = jnp.einsum(
        "hcd,hce->hde",
        key_blk * jnp.exp(last_log[:, None, :] - cum_log),
        value_blk,
        precision=highest,
    )
    new_state = jnp.exp(last_log)[:, :, None] * carry_state + fresh
    return ((new_state, offset + last_log), (result, offset[:, None, :] + cum_log))


def join_states(earlier, later):
    earlier_log, earlier_state = earlier
    later_log, later_state = later
    return (earlier_log + later_log, jnp.exp(later_log)[:, :, None] * earlier_state + later_state)


def body(
    tokens,
    in_gain,
    w_query,
    w_forget,
    w_input,
    w_outgate,
    w_conv_h,
    w_conv_b,
    w_conv_c,
    forget_floor,
    forget_leak,
    state_gain,
    conv_taps,
    group_gain,
    out_state,
    out_conv,
):
    count = tokens.shape[0]
    heads = w_query.shape[1] // GROUP_FEATURES
    channels = w_conv_h.shape[1]
    normed = rms_rows(tokens.astype(jnp.float32), in_gain).astype(jnp.bfloat16)

    def project(weight):
        return jnp.dot(normed, weight, preferred_element_type=jnp.float32).astype(jnp.bfloat16)

    proj_query = project(w_query)
    proj_forget = project(w_forget)
    proj_input = project(w_input)
    proj_outgate = project(w_outgate)
    proj_h = project(w_conv_h)
    proj_b = project(w_conv_b)
    proj_c = project(w_conv_c)
    conv_in = (proj_c.astype(jnp.float32) * proj_h.astype(jnp.float32)).astype(jnp.bfloat16)
    rim_rows = from_behind(conv_in[count - (TAPS - 1) :], "sp", 1)
    gate_logit = proj_forget.astype(jnp.float32)
    log_forget = (
        jnp.logaddexp(
            jnp.log(forget_floor), jnp.log1p(-forget_floor) + jax.nn.log_sigmoid(gate_logit)
        )
        + forget_leak
    )
    key_gate = (1.0 - forget_floor) * jax.nn.sigmoid(-gate_logit)
    query_act = jax.nn.silu(proj_query.astype(jnp.float32))
    value_f = proj_input.astype(jnp.float32)
    nblk = count // BLOCK

    def to_blocks(arr):
        return arr.reshape(nblk, BLOCK, heads, GROUP_FEATURES).transpose(0, 2, 1, 3)

    def from_blocks(arr):
        return arr.transpose(0, 2, 1, 3).reshape(count, heads, GROUP_FEATURES)

    start_state = jnp.zeros((heads, GROUP_FEATURES, GROUP_FEATURES), jnp.float32)
    start_log = jnp.zeros((heads, GROUP_FEATURES), jnp.float32)
    (local_state, total_log), (local_read, cum_blocks) = lax.scan(
        state_block,
        (start_state, start_log),
        (to_blocks(query_act), to_blocks(key_gate), to_blocks(value_f), to_blocks(log_forget)),
    )
    _, incoming = carried_in((total_log, local_state), "sp", join_states, (start_log, start_state))
    cum_device = from_blocks(cum_blocks)
    query_heads = query_act.reshape(count, heads, GROUP_FEATURES)
    cross = jnp.einsum(
        "thd,hde->the", query_heads * jnp.exp(cum_device), incoming, precision=highest
    )
    state_read = from_blocks(local_read) + cross
    out_gate = jax.nn.silu(proj_outgate.astype(jnp.float32)).reshape(count, heads, GROUP_FEATURES)
    state_res = (
        (rms_rows(state_read, state_gain) * out_gate)
        .reshape(count, heads * GROUP_FEATURES)
        .astype(jnp.bfloat16)
    )
    padded = jnp.concatenate([rim_rows, conv_in], axis=0).astype(jnp.float32)
    taps_f = conv_taps.astype(jnp.float32)
    conv_sum = jnp.zeros((count, channels), jnp.float32)
    for offset in range(TAPS):
        conv_sum = conv_sum + taps_f[offset][None, :] * padded[offset : offset + count]
    gated = (proj_b.astype(jnp.float32) * conv_sum).reshape(
        count, channels // GROUP_FEATURES, GROUP_FEATURES
    )
    conv_res = rms_rows(gated, group_gain).reshape(count, channels).astype(jnp.bfloat16)
    mixed_here = jnp.concatenate([state_res, conv_res], axis=1)
    weight_rows = jnp.concatenate([out_state, out_conv], axis=0)
    columns = lax.all_to_all(weight_rows, "tp", split_axis=1, concat_axis=0, tiled=True)
    summed = jnp.dot(
        lax.all_gather(mixed_here, "tp", axis=1, tiled=True),
        columns,
        preferred_element_type=jnp.float32,
    )
    return summed.astype(jnp.bfloat16)


def solution(mesh):
    in_specs = (
        P("sp", None),
        P(),
        P(None, "tp"),
        P(None, "tp"),
        P(None, "tp"),
        P(None, "tp"),
        P(None, "tp"),
        P(None, "tp"),
        P(None, "tp"),
        P("tp"),
        P("sp", "tp"),
        P(),
        P(None, "tp"),
        P(),
        P("tp", None),
        P("tp", None),
    )
    out_specs = P("sp", "tp")
    return jax.shard_map(body, mesh=mesh, in_specs=in_specs, out_specs=out_specs, check_vma=False)
```

profile of v0, /device:TPU:0, one launch (start us, length us, event | category | flops | bytes accessed | tf_op | source)
XLA Modules:
  0.0 359.1 jit_solution(16441014362019166451)
XLA Ops:
  6.5 3.2 fusion.21
  15.5 5.1 %collective-permute-start = (bf16[2,256]{0,1:T(8,128)(2,1)}, bf16[2,256]{0,1:T(8,128)(2,1)S(1)}, u32[]{:S(2)}, u32[]{:S(2)}) collective-permute-start(bf16[2,256]{0,1:T(8,128)(2,1)} %slice.34), channel_id=1, source_target_pairs={{0,4},{4,8},{8,12},{12,16},{16,20},{20,24},{24,28},{1,5},{5,9},{9,... | collective-permute-start | bytes 3080 | tf_op jit(solution)/shard_map/ppermute | solution.py:18
  20.6 3.5 convert_multiply_fusion.2
  24.5 5.9 %fusion.40 = (f32[1024,256]{1,0:T(8,128)}, f32[1024,256]{1,0:T(8,128)S(1)}) fusion(f32[256]{0:T(256)S(1)} %get-tuple-element.172, f32[1024,256]{1,0:T(8,128)} %param.30, f32[256]{0:T(256)S(1)} %get-tuple-element.174, f32[256]{0:T(256)S(1)} %get-tuple-element.173, bf16[1024,2048]{1,0:T(8,128)(2,1)} %copy-done.2, bf16[2048,256]{1,0:T(8,128)(2,1)S(1)} %copy-done), kind=kOutput, calls=%fused_computation.74 | convolution fusion | flops 1079771136 | bytes 8391680 | tf_op jit(solution)/shard_map/dot_general | solution.py:100
  30.4 2.8 reshape.103
  34.8 3.8 %convert_multiply_fusion.3 = f32[1024,256]{1,0:T(8,128)S(1)} fusion(bf16[1024,2048]{1,0:T(8,128)(2,1)} %copy-done.2, bf16[2048,256]{1,0:T(8,128)(2,1)} %param.22), kind=kOutput, calls=%fused_computation.48 | convolution fusion | flops 1075314688 | bytes 6291456 | tf_op jit(solution)/shard_map/dot_general | solution.py:100
  40.0 4.7 %fusion.33 = f32[1024,256]{1,0:T(8,128)} fusion(bf16[1024,2048]{1,0:T(8,128)(2,1)} %copy-done.2, bf16[2048,256]{1,0:T(8,128)(2,1)} %param.24), kind=kOutput, calls=%fused_computation.66 | convolution fusion | flops 1074266112 | bytes 6291456 | tf_op jit(solution)/shard_map/dot_general | solution.py:100
  44.7 2.7 reshape.110
  47.5 3.3 copy_bitcast_fusion.2
  52.5 177.0 %while.30 = (s32[]{:T(128)}, f32[2,128,128]{2,1,0:T(8,128)S(1)}, f32[2,128]{1,0:T(2,128)S(1)}, f32[16,2,64,128]{3,2,0,1:T(8,128)}, f32[16,2,64,128]{3,2,0,1:T(8,...) while((s32[]{:T(128)}, f32[2,128,128]{2,1,0:T(8,128)S(1)}, ...), condition=%wide.region_3.4_spmd.clone, body=%wide.region_1.3_spmd.clone.sunk | while | flops 69399040 | bytes 10310300 | solution.py:131
  57.6 3.5 fusion.89
  68.7 3.5 fusion.89
  79.7 3.5 fusion.89
  90.8 3.5 fusion.89
  101.9 3.5 fusion.89
  112.9 3.5 fusion.89
  124.0 3.5 fusion.89
  135.1 3.5 fusion.89
  146.1 3.5 fusion.89
  157.2 3.5 fusion.89
  168.3 3.5 fusion.89
  179.3 3.5 fusion.89
  190.4 3.5 fusion.89
  201.5 3.5 fusion.89
  212.5 3.5 fusion.89
  223.6 3.5 fusion.89
  229.5 2.5 copy.94
  232.1 18.7 %all-gather.2 = bf16[8,2,128]{2,1,0:T(2,128)(2,1)S(1)} all-gather(bf16[1,2,128]{2,1,0:T(2,128)(2,1)S(1)} %convert_bitcast_fusion), channel_id=2, replica_groups=mesh['sp'=8,'tp'=4] {'sp'}, dimensions={0}, use_global_device_ids=true | all-gather | bytes 4608 | tf_op jit(solution)/shard_map/all_gather | solution.py:24
  250.7 33.4 %all-gather.1 = bf16[16,128,128]{2,1,0:T(8,128)(2,1)} all-gather(bf16[2,128,128]{2,1,0:T(8,128)(2,1)S(1)} %convert_element_type.97), channel_id=3, replica_groups=mesh['sp'=8,'tp'=4] {'sp'}, dimensions={0}, use_global_device_ids=true | all-gather | bytes 589824 | tf_op jit(solution)/shard_map/all_gather | solution.py:24
  293.8 44.7 %all_to_all.19 = bf16[512,4,512]{0,2,1:T(8,128)(2,1)S(1)} all-to-all(bf16[512,4,512]{0,2,1:T(8,128)(2,1)S(1)} %bitcast.137), channel_id=1, replica_groups=mesh['sp'=8,'tp'=4] {'tp'}, dimensions={1} | all-to-all | bytes 4194304 | tf_op jit(solution)/shard_map/all_to_all | solution.py:160
  340.9 5.2 %all-gather.5.cloned.1.call-done = bf16[1024,2048]{0,1:T(8,128)(2,1)} async-done(((bf16[1024,512]{0,1:T(8,128)(2,1)}), bf16[1024,2048]{0,1:T(8,128)(2,1)}) %all-gather.5.cloned.1.call-update) | async-done | bytes 4194320 | tf_op jit(solution)/shard_map/all_gather | solution.py:162
  346.1 6.2 %convolution_convert_fusion = bf16[1024,512]{1,0:T(8,128)(2,1)} fusion(bf16[1024,2048]{0,1:T(8,128)(2,1)} %all-gather.5.cloned.1.call-done, bf16[2048,512]{1,0:T(8,128)(2,1)} %bitcast.141), kind=kOutput, calls=%fused_computation.43 | convolution fusion | flops 2148007936 | bytes 7340032 | tf_op jit(solution)/shard_map/dot_general | solution.py:161
  (248 shorter events, 142.2 us)
Async XLA Ops:
  6.5 17.9 %copy-start = (bf16[2048,256]{1,0:T(8,128)(2,1)S(1)}, bf16[2048,256]{1,0:T(8,128)(2,1)}, u32[]{:S(2)}) copy-start(bf16[2048,256]{1,0:T(8,128)(2,1)} %param.23) | copy-start | bytes 3145732
  6.5 3.2 copy-start.9
  6.5 339.5 %all-gather.5.cloned.1.call-start = ((), (), s32[]{:S(2)}) async-start(), calls=%async_computation.1 | async-start | bytes 5242880 | tf_op jit(solution)/shard_map/all_gather | solution.py:162
  6.5 3.5 copy-start.1
  10.1 1.2 copy-start.13
  11.3 2.0 copy-start.2
  11.3 2.0 copy-start.14
  13.3 7.3 %copy-start.10 = (bf16[3,256]{1,0:T(4,128)(2,1)S(1)}, bf16[3,256]{1,0:T(4,128)(2,1)}, u32[]{:S(2)}) copy-start(bf16[3,256]{1,0:T(4,128)(2,1)} %param.32) | copy-start | bytes 4612
  13.3 7.3 %copy-start.15 = (bf16[2048,256]{1,0:T(8,128)(2,1)S(1)}, bf16[2048,256]{1,0:T(8,128)(2,1)}, u32[]{:S(2)}) copy-start(bf16[2048,256]{1,0:T(8,128)(2,1)} %param.25) | copy-start | bytes 3145732
  14.6 0.8 copy-start.7
  15.5 273.0 %collective-permute-start = (bf16[2,256]{0,1:T(8,128)(2,1)}, bf16[2,256]{0,1:T(8,128)(2,1)S(1)}, u32[]{:S(2)}, u32[]{:S(2)}) collective-permute-start(bf16[2,256]{0,1:T(8,128)(2,1)} %slice.34), channel_id=1, source_target_pairs={{0,4},{4,8},{8,12},{12,16},{16,20},{20,24},{24,28},{1,5},{5,9},{9,... | collective-permute-start | bytes 3080 | tf_op jit(solution)/shard_map/ppermute | solution.py:18
  20.6 3.8 %copy-start.11 = (f32[256]{0:T(256)S(1)}, f32[256]{0:T(256)}, u32[]{:S(2)}) copy-start(f32[256]{0:T(256)} %param.29) | copy-start | bytes 3076
  47.5 3.3 copy-start.4
  47.5 3.3 copy-start.5
  284.2 4.1 %copy-start.12 = (f32[128]{0:T(128)S(1)}, f32[128]{0:T(128)}, u32[]{:S(2)}) copy-start(f32[128]{0:T(128)} %param.31) | copy-start | bytes 1540
  284.2 4.2 %copy-start.17 = (f32[128]{0:T(128)S(1)}, f32[128]{0:T(128)}, u32[]{:S(2)}) copy-start(f32[128]{0:T(128)} %param.33) | copy-start | bytes 1540
  284.2 4.2 %copy-start.8 = (bf16[1024,256]{0,1:T(8,128)(2,1)S(1)}, bf16[1024,256]{0,1:T(8,128)(2,1)}, u32[]{:S(2)}) copy-start(bf16[1024,256]{0,1:T(8,128)(2,1)} %copy-done.7) | copy-start | bytes 1572868
  285.6 3.1 copy-start.3
  285.7 3.1 copy-start.16
  290.3 1.3 copy-start.6
Sparse Core Ops, SparseCore 0:
  291.7 54.3 all-gather.4
where the time goes:
time: 366 us; the launch traced here: 359 us
  matrix products  97.1 us (27%)
  blocking collectives  96.8 us (26%)
  other arithmetic  88.3 us (24%)
  local copies, waits for them, and re-layouts  52.1 us (14%)
  between operations  13.8 us (4%)
  waiting for transfers between devices  5.25 us (1%)
  starting transfers between devices  5.07 us (1%)
    dot_general x16, other arithmetic, state_block(): jnp.einsum('hid,hjd,hijd->hij', query_blk, key_blk, decay_all, precision=...  56.6 us
    all_gather x2, blocking collectives, carried_in(): lax.all_gather(a.astype(kind), axis)  52.1 us
    all_to_all x1, blocking collectives, body(): lax.all_to_all(weight_rows, 'tp', split_axis=1, concat_axis=0, tiled=True)  44.7 us
    dot_general x16, matrix products, state_block(): jnp.einsum('hij,hje->hie', scores, value_blk, precision=highest)  28.3 us
    squeeze x32, local copies, waits for them, and re-layouts, body(): lax.scan(state_block, (start_state, start_log), (to_blocks(query_act), to...  27.7 us
    dot_general x7, matrix products, project(): jnp.dot(normed, weight, preferred_element_type=jnp.float32)  22.1 us
    dot_general x16, matrix products, state_block(): jnp.einsum('hcd,hce->hde', key_blk * jnp.exp(last_log[:, None, :] - cum_l...  20.5 us
    dot_general x16, matrix products, state_block(): jnp.einsum('hcd,hde->hce', query_blk * jnp.exp(cum_log), carry_state, pre...  17.5 us
  transfers between devices with their start and end apart: 2, of which 1 were waited for; matrix products, arithmetic and copies ran while one was open for 61% of the time, Pallas kernels for 0%

commit v1 on v0

v1 whole, which is shorter than its diff:
```python
import functools

import jax
import jax.numpy as jnp
from jax import lax
from jax.experimental import pallas as pl
from jax.experimental.pallas import tpu as pltpu
from jax.sharding import PartitionSpec as P

GROUP_FEATURES = 128
CHUNK = 128
ROWS = 256
TAPS = 3
HALO = 8

norm_eps = 1e-06
f32 = jnp.float32
bf16 = jnp.bfloat16


def dot(a, b, dims=((1,), (0,)), precision=None):
    return lax.dot_general(a, b, (dims, ((), ())), precision=precision, preferred_element_type=f32)


def rms(values):
    return values * lax.rsqrt(jnp.mean(values * values, axis=-1, keepdims=True) + norm_eps)


def per_group(values, gain):
    parts = []
    for g in range(values.shape[1] // GROUP_FEATURES):
        parts.append(rms(values[:, g * GROUP_FEATURES : (g + 1) * GROUP_FEATURES]) * gain)
    return jnp.concatenate(parts, axis=1)


def local_kernel(
    tokens, in_gain, wq, wf, wi, wg, wh, wb, wc, floor, leak, taps, group_gain,
    read_out, qdev_out, gate_out, conv_out, state_out, log_out, conv_tail, head_conv, head_gate,
    pad, state, offset,
):
    step = pl.program_id(0)
    rows = tokens.shape[0]

    @pl.when(step == 0)
    def _():
        pad[0:HALO, :] = jnp.zeros((HALO, pad.shape[1]), f32)
        state[...] = jnp.zeros_like(state)
        offset[...] = jnp.zeros_like(offset)

    normed = (rms(tokens[...].astype(f32)) * in_gain[...]).astype(bf16)

    def project(w):
        return dot(normed, w[...]).astype(bf16).astype(f32)

    conv_in = (project(wc) * project(wh)).astype(bf16).astype(f32)
    proj_b = project(wb)
    pad[HALO : HALO + rows, :] = conv_in
    t = taps[...].astype(f32)
    total = t[TAPS - 1 : TAPS] * conv_in
    for j in range(TAPS - 1):
        total += t[j : j + 1] * pad[HALO - (TAPS - 1) + j : HALO - (TAPS - 1) + j + rows, :]
    conv_out[...] = per_group(proj_b * total, group_gain[...]).astype(bf16)

    @pl.when(step == 0)
    def _():
        head_conv[...] = conv_in[:HALO].astype(bf16)
        head_gate[...] = proj_b[:HALO].astype(bf16)

    tail = conv_in[rows - HALO :]
    pad[0:HALO, :] = tail
    conv_tail[...] = tail.astype(bf16)

    x = project(wf)
    key = (1.0 - floor[...]) * jax.nn.sigmoid(-x)
    logf = jnp.log(1.0 - key) + leak[...]
    value = dot(normed, wi[...]).astype(bf16)
    query = jax.nn.silu(project(wq))
    gate_out[...] = dot(normed, wg[...]).astype(bf16)

    r = lax.broadcasted_iota(jnp.int32, (CHUNK, CHUNK), 0)
    c = lax.broadcasted_iota(jnp.int32, (CHUNK, CHUNK), 1)
    causal = r >= c
    ones = causal.astype(f32)
    for b in range(rows // CHUNK):
        lo, hi = b * CHUNK, (b + 1) * CHUNK
        cum = dot(ones, logf[lo:hi], precision=lax.Precision.HIGHEST)
        mid = cum[CHUNK // 2 - 1 : CHUNK // 2]
        last = cum[CHUNK - 1 : CHUNK]
        q_mid = query[lo:hi] * jnp.exp(cum - mid)
        k_mid = key[lo:hi] * jnp.exp(mid - cum)
        q_all = q_mid * jnp.exp(mid)
        k_end = (k_mid * jnp.exp(last - mid)).astype(bf16)
        qdev_out[lo:hi, :] = (q_all * jnp.exp(offset[...])).astype(bf16)
        q_mid, k_mid, q_all = q_mid.astype(bf16), k_mid.astype(bf16), q_all.astype(bf16)
        for h in range(value.shape[1] // GROUP_FEATURES):
            s = slice(h * GROUP_FEATURES, (h + 1) * GROUP_FEATURES)
            scores = dot(q_mid[:, s], k_mid[:, s], ((1,), (1,)))
            scores = jnp.where(causal, scores, 0.0).astype(bf16)
            v = value[lo:hi, s]
            held = state[h]
            read_out[lo:hi, s] = dot(scores, v) + dot(q_all[:, s], held.astype(bf16), ((1,), (1,)))
            state[h] = held * jnp.exp(last[:, s]) + dot(v, k_end[:, s], ((0,), (0,)))
        offset[...] += last
    state_out[...] = state[...].astype(bf16)
    log_out[...] = offset[...]


def merge_kernel(
    read, qdev, gate, conv, states, logs, rim, head_conv, head_gate, state_gain, group_gain, taps,
    mixed, incoming,
):
    place = lax.axis_index("sp")
    heads, rows = states.shape[1], read.shape[0]

    @pl.when(pl.program_id(0) == 0)
    def _():
        incoming[...] = jnp.zeros_like(incoming)

        def hop(p, _):
            decay = jnp.exp(logs[pl.ds(p, 1)][0])
            for h in range(heads):
                s = slice(h * GROUP_FEATURES, (h + 1) * GROUP_FEATURES)
                incoming[h] = incoming[h] * decay[:, s] + states[pl.ds(p, 1)][0, h].astype(f32)
            return 0

        lax.fori_loop(0, place, hop, 0)

    width = heads * GROUP_FEATURES
    for h in range(heads):
        s = slice(h * GROUP_FEATURES, (h + 1) * GROUP_FEATURES)
        whole = read[:, s] + dot(qdev[:, s], incoming[h].astype(bf16), ((1,), (1,)))
        out = rms(whole) * state_gain[...] * jax.nn.silu(gate[:, s].astype(f32))
        mixed[:, s] = out.astype(bf16)
    mixed[:, width:] = conv[...]

    @pl.when(pl.program_id(0) == 0)
    def _():
        t = taps[...].astype(f32)
        own = head_conv[...].astype(f32)
        ext = jnp.concatenate([rim[...].astype(f32), own], axis=0)
        total = t[TAPS - 1 : TAPS] * own
        for j in range(TAPS - 1):
            total += t[j : j + 1] * ext[HALO - (TAPS - 1) + j : 2 * HALO - (TAPS - 1) + j]
        fixed = per_group(head_gate[...].astype(f32) * total, group_gain[...])
        mixed[0:HALO, width:] = fixed.astype(bf16)


def body(
    tokens, in_gain, w_query, w_forget, w_input, w_outgate, w_conv_h, w_conv_b, w_conv_c,
    forget_floor, forget_leak, state_gain, conv_taps, group_gain, out_state, out_conv,
):
    count, feats = tokens.shape
    width, channels = w_query.shape[1], w_conv_h.shape[1]
    heads = width // GROUP_FEATURES
    weight_rows = jnp.concatenate([out_state, out_conv], axis=0)
    columns = lax.all_to_all(weight_rows, "tp", split_axis=1, concat_axis=0, tiled=True)

    def whole(shape):
        return pl.BlockSpec(shape, lambda i: (0,) * len(shape))

    def rows(n):
        return pl.BlockSpec((ROWS, n), lambda i: (i, 0))

    read, qdev, gate, conv, state, log, tail, head_conv, head_gate = pl.pallas_call(
        local_kernel,
        grid=(count // ROWS,),
        in_specs=[rows(feats), whole((1, feats))] + [whole((feats, width))] * 4
        + [whole((feats, channels))] * 3
        + [whole((1, width)), rows(width), whole((TAPS, channels)), whole((1, GROUP_FEATURES))],
        out_specs=[
            rows(width), rows(width), rows(width), rows(channels),
            whole((heads, GROUP_FEATURES, GROUP_FEATURES)), whole((1, width)),
            whole((HALO, channels)), whole((HALO, channels)), whole((HALO, channels)),
        ],
        out_shape=[
            jax.ShapeDtypeStruct((count, width), f32),
            jax.ShapeDtypeStruct((count, width), bf16),
            jax.ShapeDtypeStruct((count, width), bf16),
            jax.ShapeDtypeStruct((count, channels), bf16),
            jax.ShapeDtypeStruct((heads, GROUP_FEATURES, GROUP_FEATURES), bf16),
            jax.ShapeDtypeStruct((1, width), f32),
            jax.ShapeDtypeStruct((HALO, channels), bf16),
            jax.ShapeDtypeStruct((HALO, channels), bf16),
            jax.ShapeDtypeStruct((HALO, channels), bf16),
        ],
        scratch_shapes=[
            pltpu.VMEM((HALO + ROWS, channels), f32),
            pltpu.VMEM((heads, GROUP_FEATURES, GROUP_FEATURES), f32),
            pltpu.VMEM((1, width), f32),
        ],
        compiler_params=pltpu.CompilerParams(vmem_limit_bytes=48 * 2**20),
        cost_estimate=pl.CostEstimate(
            flops=2 * count * feats * (4 * width + 3 * channels),
            bytes_accessed=2 * feats * (count + 4 * width + 3 * channels),
            transcendentals=8 * count * width,
        ),
    )(
        tokens, in_gain[None], w_query, w_forget, w_input, w_outgate, w_conv_h, w_conv_b, w_conv_c,
        forget_floor[None], forget_leak, conv_taps, group_gain[None],
    )
    size = lax.axis_size("sp")
    rim = lax.ppermute(tail, "sp", [(i, i + 1) for i in range(size - 1)])
    states = lax.all_gather(state, "sp")
    logs = lax.all_gather(log, "sp")
    mixed = pl.pallas_call(
        merge_kernel,
        grid=(count // ROWS,),
        in_specs=[
            rows(width), rows(width), rows(width), rows(channels), whole(states.shape), whole(logs.shape),
            whole(rim.shape), whole(rim.shape), whole(rim.shape),
            whole((1, GROUP_FEATURES)), whole((1, GROUP_FEATURES)), whole((TAPS, channels)),
        ],
        out_specs=rows(width + channels),
        out_shape=jax.ShapeDtypeStruct((count, width + channels), bf16),
        scratch_shapes=[pltpu.VMEM((heads, GROUP_FEATURES, GROUP_FEATURES), f32)],
        compiler_params=pltpu.CompilerParams(vmem_limit_bytes=32 * 2**20),
    )(
        read, qdev, gate, conv, states, logs, rim, head_conv, head_gate,
        state_gain[None], group_gain[None], conv_taps,
    )
    everything = lax.all_gather(mixed, "tp", axis=1, tiled=True)
    return jnp.dot(everything, columns, preferred_element_type=f32).astype(bf16)


def solution(mesh):
    cols, rows = P(None, "tp"), P("tp", None)
    in_specs = (
        P("sp", None), P(), cols, cols, cols, cols, cols, cols, cols,
        P("tp"), P("sp", "tp"), P(), cols, P(), rows, rows,
    )
    return jax.shard_map(
        body, mesh=mesh, in_specs=in_specs, out_specs=P("sp", "tp"), check_vma=False
    )
```

time: 366 us -> 158 us (0.43); the launches traced: 359 us -> 158 us
  matrix products: 97.1 us -> 6.16 us
  other arithmetic: 88.3 us -> 0.16 us
  local copies, waits for them, and re-layouts: 52.1 us -> 10.5 us
  Pallas kernels: 0 us -> 21.9 us
  waiting for transfers between devices: 5.25 us -> 0.02 us
  blocking collectives: 96.8 us -> 101 us
    dot_general x57 -> x1, matrix products: 97.1 us -> 6.16 us  [body(): return jnp.dot(everything, columns, preferred_element_type=f32).astype(bf16)]
    dot_general x16 -> x0, other arithmetic: 56.6 us -> none  [state_block(): jnp.einsum('hid,hjd,hijd->hij', query_blk, key_blk, decay_all, precision=...]
    squeeze x32 -> x0, local copies, waits for them, and re-layouts: 27.7 us -> none  [body(): lax.scan(state_block, (start_state, start_log), (to_blocks(query_act), to...]
    pallas_call x0 -> x2, Pallas kernels: none -> 21.9 us  [the longest x1 19.4 us: body(): pl.pallas_call(local_kernel, grid=(count // ROWS,), in_specs=[rows(feats)...]
    exp x16 -> x0, other arithmetic: 13.4 us -> none  [state_block(): decay_all = jnp.exp(jnp.where(causal, diff_log, -jnp.inf))]
    dynamic_update_slice x16 -> x0, other arithmetic: 10.1 us -> none  [body(): lax.scan(state_block, (start_state, start_log), (to_blocks(query_act), to...]
    reshape x5 -> x0, local copies, waits for them, and re-layouts: 8.71 us -> none  [the longest x3 5.84 us: to_blocks(): return arr.reshape(nblk, BLOCK, heads, GROUP_FEATURES).transpose(0, 2, 1, 3)]
    transpose x3 -> x0, local copies, waits for them, and re-layouts: 7.73 us -> none  [to_blocks(): return arr.reshape(nblk, BLOCK, heads, GROUP_FEATURES).transpose(0, 2, 1, 3)]
  transfers between devices with their start and end apart: 2 -> 2, of which waited for: 1 -> 0; matrix products, arithmetic and copies ran while one was open for 61% -> 2% of each run, Pallas kernels for 0% -> 0%
where the time goes in v1:
time: 158 us
  blocking collectives  101 us (64%)
  Pallas kernels  21.9 us (14%)
  between operations  13.5 us (9%)
  local copies, waits for them, and re-layouts  10.5 us (7%)
  matrix products  6.16 us (4%)
  starting transfers between devices  4.87 us (3%)
    all_to_all x1, blocking collectives, body(): lax.all_to_all(weight_rows, 'tp', split_axis=1, concat_axis=0, tiled=True)  50.7 us
    all_gather x1, blocking collectives, body(): states = lax.all_gather(state, 'sp')  31.9 us
    pallas_call x1, Pallas kernels, body(): pl.pallas_call(local_kernel, grid=(count // ROWS,), in_specs=[rows(feats)...  19.4 us
    all_gather x1, blocking collectives, body(): logs = lax.all_gather(log, 'sp')  18.2 us
    unnamed x22, local copies, waits for them, and re-layouts  8.09 us
    dot_general x1, matrix products, body(): return jnp.dot(everything, columns, preferred_element_type=f32).astype(bf16)  6.16 us
    ppermute x1, starting transfers between devices, body(): rim = lax.ppermute(tail, 'sp', [(i, i + 1) for i in range(size - 1)])  4.87 us
  transfers between devices with their start and end apart: 2, of which 0 were waited for; matrix products, arithmetic and copies ran while one was open for 2% of the time, Pallas kernels for 0%

profile of v1, /device:TPU:0, one launch (start us, length us, event | category | flops | bytes accessed | tf_op | source)
XLA Modules:
  0.0 157.8 jit_solution(14576035068411700213)
XLA Ops:
  6.5 0.0 all-gather.5.cloned.1.call-start
  6.5 0.0 copy-start
  6.5 0.7 copy-done
  7.2 0.0 copy-start.1
  7.2 0.7 copy-done.1
  7.9 0.0 copy-start.3
  7.9 1.2 copy-done.3
  9.1 0.0 copy-start.4
  9.1 1.2 copy-done.4
  10.3 0.0 copy-start.5
  10.3 1.2 copy-done.5
  11.6 0.0 copy-start.6
  11.6 0.7 copy-done.6
  12.2 0.0 copy-start.7
  12.3 0.7 copy-done.7
  12.9 0.0 copy-start.2
  12.9 19.4 %shard_map.154 = (f32[1024,256]{1,0:T(8,128)S(1)}, bf16[1024,256]{1,0:T(8,128)(2,1)S(1)}, bf16[1024,256]{1,0:T(8,128)(2,1)S(1)}, bf16[1024,256]{1,0:T(8,128)(2,1...) custom-call(bf16[1024,2048]{1,0:T(8,128)(2,1)} %tokens.1, ...), custom_call_target="tpu_custom_call" | custom-call | flops 7516192768 | bytes 11534336 | tf_op jit(solution)/shard_map/pallas_call | solution.py:164
  32.3 4.9 %collective-permute-start = (bf16[8,256]{1,0:T(8,128)(2,1)S(1)}, bf16[8,256]{1,0:T(8,128)(2,1)S(1)}, u32[]{:S(2)}, u32[]{:S(2)}) collective-permute-start(bf16[8,256]{1,0:T(8,128)(2,1)S(1)} %get-tuple-element.20), channel_id=1, source_target_pairs={{0,4},{4,8},{8,12},{12,16},{16,20},{20,24},{24,28},{1,5},{5,9},{9,... | collective-permute-start | bytes 12296 | tf_op jit(solution)/shard_map/ppermute | solution.py:202
  37.2 31.9 %all-gather = bf16[16,128,128]{2,1,0:T(8,128)(2,1)S(1)} all-gather(bf16[2,128,128]{2,1,0:T(8,128)(2,1)S(1)} %get-tuple-element.18), channel_id=2, replica_groups=mesh['sp'=8,'tp'=4] {'sp'}, dimensions={0}, use_global_device_ids=true | all-gather | bytes 589824 | tf_op jit(solution)/shard_map/all_gather | solution.py:203
  69.1 18.2 %all-gather.2.logs = f32[8,1,256]{2,1,0:T(1,128)S(1)} all-gather(f32[1,1,256]{2,1,0:T(1,128)S(1)} %bitcast.12), channel_id=3, replica_groups=mesh['sp'=8,'tp'=4] {'sp'}, dimensions={0}, use_global_device_ids=true | all-gather | bytes 9216 | tf_op jit(solution)/shard_map/all_gather | solution.py:204
  87.3 0.0 collective-permute-done.rim
  87.3 0.0 copy-done.2
  87.3 2.5 %shard_map.155 = bf16[1024,512]{1,0:T(8,128)(2,1)} custom-call(f32[1024,256]{1,0:T(8,128)S(1)} %get-tuple-element.14.read, bf16[1024,256]{1,0:T(8,128)(2,1)S(1)} %get-tuple-element.15.qdev, bf16[1024,256]{1,0:T(8,128)(2,1)S(1)} %get-tuple-element.16.gate, bf16[1024,256]{1,0:T(8,128)(2,1)S(1)} %get-tuple-element.17.conv, ...), custom_call_target="tpu_custom_call" | custom-call | tf_op jit(solution)/shard_map/pallas_call | solution.py:205
  89.8 0.0 all-gather.5.cloned.1.call-update
  89.8 0.0 copy-done.8
  89.9 0.5 copy.20
  90.4 0.7 copy-done.9
  91.0 0.5 copy.21
  91.6 0.2 pad_maximum_fusion
  91.7 50.7 %all_to_all.19 = bf16[512,4,512]{0,2,1:T(8,128)(2,1)S(1)} all-to-all(bf16[512,4,512]{0,2,1:T(8,128)(2,1)S(1)} %bitcast.18), channel_id=1, replica_groups=mesh['sp'=8,'tp'=4] {'tp'}, dimensions={1} | all-to-all | bytes 4194304 | tf_op jit(solution)/shard_map/all_to_all | solution.py:156
  142.4 2.4 %copy.22 = bf16[4,512,512]{2,1,0:T(8,128)(2,1)} copy(bf16[4,512,512]{1,2,0:T(8,128)(2,1)S(1)} %bitcast.19) | data formatting | bytes 4194304 | tf_op jit(solution)/shard_map/all_to_all | solution.py:156
  144.8 6.2 %convolution_convert_fusion = bf16[1024,512]{1,0:T(8,128)(2,1)} fusion(bf16[1024,2048]{1,0:T(8,128)(2,1)} %all-gather.5.cloned.1.call-done, bf16[2048,512]{1,0:T(8,128)(2,1)} %bitcast.20), kind=kOutput, calls=%fused_computation.1 | convolution fusion | flops 2148007936 | bytes 7340032 | tf_op jit(solution)/shard_map/dot_general | solution.py:222
  (3 shorter events, 0.0 us)
Async XLA Ops:
  6.5 138.2 %all-gather.5.cloned.1.call-start = ((), (), s32[]{:S(2)}) async-start(), calls=%async_computation.1 | async-start | bytes 5242880 | tf_op jit(solution)/shard_map/all_gather | solution.py:221
  6.5 0.7 copy-start
  7.2 0.7 copy-start.1
  7.9 1.2 copy-start.3
  9.1 1.2 copy-start.4
  10.3 1.2 copy-start.5
  11.6 0.7 copy-start.6
  12.2 0.7 copy-start.7
  12.9 74.3 %copy-start.2 = (f32[128]{0:T(128)S(1)}, f32[128]{0:T(128)}, u32[]{:S(2)}) copy-start(f32[128]{0:T(128)} %param.27) | copy-start | bytes 1540
  32.3 54.9 %collective-permute-start = (bf16[8,256]{1,0:T(8,128)(2,1)S(1)}, bf16[8,256]{1,0:T(8,128)(2,1)S(1)}, u32[]{:S(2)}, u32[]{:S(2)}) collective-permute-start(bf16[8,256]{1,0:T(8,128)(2,1)S(1)} %get-tuple-element.20), channel_id=1, source_target_pairs={{0,4},{4,8},{8,12},{12,16},{16,20},{20,24},{24,28},{1,5},{5,9},{9,... | collective-permute-start | bytes 12296 | tf_op jit(solution)/shard_map/ppermute | solution.py:202
  87.3 2.6 %copy-start.8 = (bf16[256,2048]{1,0:T(8,128)(2,1)S(1)}, bf16[256,2048]{1,0:T(8,128)(2,1)}, u32[]{:S(2)}) copy-start(bf16[256,2048]{1,0:T(8,128)(2,1)} %param.30) | copy-start | bytes 3145732
  89.8 1.2 copy-start.9
Sparse Core Ops, SparseCore 0:
  90.0 53.9 all-gather.4

commit v2 on v1

v2 whole, which is shorter than its diff:
```python
import functools

import jax
import jax.numpy as jnp
from jax import lax
from jax.experimental import pallas as pl
from jax.experimental.pallas import tpu as pltpu
from jax.sharding import PartitionSpec as P

GROUP_FEATURES = 128
CHUNK = 128
ROWS = 256
TAPS = 3
HALO = 8

norm_eps = 1e-06
f32 = jnp.float32
bf16 = jnp.bfloat16


def dot(a, b, dims=((1,), (0,)), precision=None):
    return lax.dot_general(a, b, (dims, ((), ())), precision=precision, preferred_element_type=f32)


def rms(values):
    return values * lax.rsqrt(jnp.mean(values * values, axis=-1, keepdims=True) + norm_eps)


def per_group(values, gain):
    parts = []
    for g in range(values.shape[1] // GROUP_FEATURES):
        parts.append(rms(values[:, g * GROUP_FEATURES : (g + 1) * GROUP_FEATURES]) * gain)
    return jnp.concatenate(parts, axis=1)


def fused_kernel(
    tp, sp,
    tokens, in_gain, wq, wf, wi, wg, wh, wb, wc, floor, leak, state_gain, taps, group_gain,
    out_state, out_conv, result,
    pad, state, offset, read, qdev, gate, conv_all, mix_all, columns, states, logs, sent_state,
    rim, tail, head_conv, head_gate, incoming,
    col_send, col_recv, own_sem, blk_send, fwd_send, blk_recv, st_send, st_recv, log_send, log_recv,
    rim_send, rim_recv,
):
    step, steps = pl.program_id(0), pl.num_programs(0)
    rows = tokens.shape[0]
    me, place = lax.axis_index("tp"), lax.axis_index("sp")
    partner = me + 1 - 2 * lax.rem(me, 2)
    ncols = result.shape[1]
    heads = state.shape[0]
    here = pl.ds(pl.multiple_of(step * rows, rows), rows)
    held = (conv_all, mix_all)

    def col_copy(kind, k):
        target = lax.rem(me + k, tp)
        src = (out_state, out_conv)[kind].at[:, pl.ds(pl.multiple_of(target * ncols, ncols), ncols)]
        dst = columns.at[kind, me]
        if k == 0:
            return pltpu.make_async_copy(src, dst, own_sem.at[kind])
        return pltpu.make_async_remote_copy(
            src, dst, col_send.at[kind, k], col_recv.at[kind, me], device_id={"tp": target}
        )

    def block_copy(kind, t, origin, target, send):
        ref = held[kind].at[origin, t]
        return pltpu.make_async_remote_copy(
            ref, ref, send, blk_recv.at[kind, origin, t], device_id={"tp": target}
        )

    def own_copies(kind, t):
        out = [block_copy(kind, t, me, partner, blk_send.at[kind, 0, t])]
        for k in range(1, tp // 2):
            out.append(block_copy(kind, t, me, lax.rem(me + 2 * k, tp), blk_send.at[kind, k, t]))
        return out

    def relays(kind, t):
        out = []
        for k in range(1, tp // 2):
            origin = lax.rem(me + 2 * k, tp)
            out.append(block_copy(kind, t, origin, partner, fwd_send.at[kind, k, t]))
        return out

    def state_copies(k):
        target = lax.rem(place + k, sp)
        to = {"sp": target}
        return (
            pltpu.make_async_remote_copy(
                sent_state, states.at[place], st_send.at[k], st_recv.at[place], device_id=to
            ),
            pltpu.make_async_remote_copy(
                offset, logs.at[place], log_send.at[k], log_recv.at[place], device_id=to
            ),
        )

    def state_arrivals(k):
        source = lax.rem(place + k, sp)
        to = {"sp": source}
        return (
            pltpu.make_async_remote_copy(
                sent_state, states.at[source], st_send.at[k], st_recv.at[source], device_id=to
            ),
            pltpu.make_async_remote_copy(
                offset, logs.at[source], log_send.at[k], log_recv.at[source], device_id=to
            ),
        )

    rim_copy = pltpu.make_async_remote_copy(
        tail, rim, rim_send.at[0], rim_recv.at[0], device_id={"sp": lax.rem(place + 1, sp)}
    )

    @pl.when(step == 0)
    def _():
        barrier = pltpu.get_barrier_semaphore()
        for k in range(1, tp):
            pl.semaphore_signal(barrier, inc=1, device_id={"tp": lax.rem(me + k, tp)})
        for k in range(1, sp):
            pl.semaphore_signal(barrier, inc=1, device_id={"sp": lax.rem(place + k, sp)})
        pl.semaphore_wait(barrier, tp + sp - 2)
        for kind in (1, 0):
            for k in range(tp):
                col_copy(kind, k).start()
        pad[0:HALO, :] = jnp.zeros((HALO, pad.shape[1]), f32)
        state[...] = jnp.zeros_like(state)
        offset[...] = jnp.zeros_like(offset)

    normed = (rms(tokens[...].astype(f32)) * in_gain[...]).astype(bf16)

    def project(w):
        return dot(normed, w[...]).astype(bf16).astype(f32)

    conv_in = (project(wc) * project(wh)).astype(bf16).astype(f32)
    proj_b = project(wb)
    pad[HALO : HALO + rows, :] = conv_in
    w = taps[...].astype(f32)
    total = w[TAPS - 1 : TAPS] * conv_in
    for j in range(TAPS - 1):
        total += w[j : j + 1] * pad[HALO - (TAPS - 1) + j : HALO - (TAPS - 1) + j + rows, :]
    conv_all[me, step] = per_group(proj_b * total, group_gain[...]).astype(bf16)

    @pl.when(step == 0)
    def _():
        head_conv[...] = conv_in[:HALO]
        head_gate[...] = proj_b[:HALO]

    pad[0:HALO, :] = conv_in[rows - HALO :]

    x = project(wf)
    key = (1.0 - floor[...]) * jax.nn.sigmoid(-x)
    logf = jnp.log(1.0 - key) + leak[...]
    value = dot(normed, wi[...]).astype(bf16)
    query = jax.nn.silu(project(wq))
    gate[here, :] = dot(normed, wg[...]).astype(bf16)

    r = lax.broadcasted_iota(jnp.int32, (CHUNK, CHUNK), 0)
    c = lax.broadcasted_iota(jnp.int32, (CHUNK, CHUNK), 1)
    causal = r >= c
    ones = causal.astype(f32)
    for b in range(rows // CHUNK):
        lo, hi = b * CHUNK, (b + 1) * CHUNK
        at = pl.ds(pl.multiple_of(step * rows + lo, CHUNK), CHUNK)
        cum = dot(ones, logf[lo:hi], precision=lax.Precision.HIGHEST)
        mid = cum[CHUNK // 2 - 1 : CHUNK // 2]
        last = cum[CHUNK - 1 : CHUNK]
        q_mid = query[lo:hi] * jnp.exp(cum - mid)
        k_mid = key[lo:hi] * jnp.exp(mid - cum)
        q_all = q_mid * jnp.exp(mid)
        k_end = (k_mid * jnp.exp(last - mid)).astype(bf16)
        qdev[at, :] = (q_all * jnp.exp(offset[0:1, :])).astype(bf16)
        q_mid, k_mid, q_all = q_mid.astype(bf16), k_mid.astype(bf16), q_all.astype(bf16)
        for h in range(heads):
            s = slice(h * GROUP_FEATURES, (h + 1) * GROUP_FEATURES)
            scores = dot(q_mid[:, s], k_mid[:, s], ((1,), (1,)))
            scores = jnp.where(causal, scores, 0.0).astype(bf16)
            v = value[lo:hi, s]
            old = state[h]
            read[at, s] = dot(scores, v) + dot(q_all[:, s], old.astype(bf16), ((1,), (1,)))
            state[h] = old * jnp.exp(last[:, s]) + dot(v, k_end[:, s], ((0,), (0,)))
        offset[...] += last

    @pl.when(step > 0)
    def _():
        for copy in own_copies(0, step):
            copy.start()

    @pl.when(step == steps - 1)
    def _():
        nb = read.shape[0] // rows
        tail[...] = pad[0:HALO, :]
        sent_state[...] = state[...].astype(bf16)
        rim_copy.start()
        for k in range(1, sp):
            for copy in state_copies(k):
                copy.start()
        rim_copy.wait_recv()
        before = jnp.where(place > 0, rim[...], 0.0)
        ext = jnp.concatenate([before, head_conv[...]], axis=0)
        fixed = w[TAPS - 1 : TAPS] * head_conv[...]
        for j in range(TAPS - 1):
            fixed += w[j : j + 1] * ext[HALO - (TAPS - 1) + j : 2 * HALO - (TAPS - 1) + j]
        fixed = per_group(head_gate[...] * fixed, group_gain[...])
        conv_all[me, 0, 0:HALO, :] = fixed.astype(bf16)

        for k in range(1, sp):
            for copy in state_arrivals(k):
                copy.wait_recv()
        for copy in own_copies(0, 0):
            copy.start()
        incoming[...] = jnp.zeros_like(incoming)

        def hop(p, _):
            decay = jnp.exp(logs[p, 0:1, :])
            for h in range(heads):
                s = slice(h * GROUP_FEATURES, (h + 1) * GROUP_FEATURES)
                incoming[h] = incoming[h] * decay[:, s] + states[p, h].astype(f32)
            return 0

        lax.fori_loop(0, place, hop, 0)

        def merge(t, _):
            at = pl.ds(pl.multiple_of(t * rows, rows), rows)
            for h in range(heads):
                s = slice(h * GROUP_FEATURES, (h + 1) * GROUP_FEATURES)
                whole = read[at, s] + dot(qdev[at, s], incoming[h].astype(bf16), ((1,), (1,)))
                out = rms(whole) * state_gain[...] * jax.nn.silu(gate[at, s].astype(f32))
                mix_all[me, t, :, s] = out.astype(bf16)
            for copy in own_copies(1, t):
                copy.start()
            return 0

        lax.fori_loop(0, nb, merge, 0)

        def relay(kind, t):
            for copy in relays(kind, t):
                copy.wait_recv()
                copy.start()

        def conv_relay(t, _):
            relay(0, t + 1)
            return 0

        lax.fori_loop(0, nb - 1, conv_relay, 0)
        relay(0, 0)
        for kind in range(2):
            col_copy(kind, 0).wait()
            for k in range(1, tp):
                source = lax.rem(me + k, tp)
                ref = columns.at[kind, source]
                pltpu.make_async_remote_copy(
                    ref, ref, col_send.at[kind, k], col_recv.at[kind, source],
                    device_id={"tp": source},
                ).wait_recv()

        def finish(t, _):
            relay(1, t)
            for kind in range(2):
                for k in range(tp // 2):
                    origin = lax.rem(partner + 2 * k, tp)
                    block_copy(kind, t, origin, partner, blk_send.at[kind, 0, t]).wait_recv()
            acc = jnp.zeros((rows, ncols), f32)
            for o in range(tp):
                acc += dot(mix_all[o, t], columns[0, o])
                acc += dot(conv_all[o, t], columns[1, o])
            result[pl.ds(pl.multiple_of(t * rows, rows), rows), :] = acc.astype(bf16)
            return 0

        lax.fori_loop(0, nb, finish, 0)

        def drain(t, _):
            for kind in range(2):
                for copy in own_copies(kind, t) + relays(kind, t):
                    copy.wait_send()
            return 0

        lax.fori_loop(0, nb, drain, 0)
        for kind in range(2):
            for k in range(1, tp):
                col_copy(kind, k).wait_send()
        rim_copy.wait_send()
        for k in range(1, sp):
            for copy in state_copies(k):
                copy.wait_send()


def body(
    tokens, in_gain, w_query, w_forget, w_input, w_outgate, w_conv_h, w_conv_b, w_conv_c,
    forget_floor, forget_leak, state_gain, conv_taps, group_gain, out_state, out_conv,
):
    count, feats = tokens.shape
    width, channels = w_query.shape[1], w_conv_h.shape[1]
    heads = width // GROUP_FEATURES
    tp, sp = lax.axis_size("tp"), lax.axis_size("sp")
    ncols, nb = out_state.shape[1] // tp, count // ROWS

    def whole(*shape):
        return pl.BlockSpec(shape, lambda i: (0,) * len(shape))

    def rows(n):
        return pl.BlockSpec((ROWS, n), lambda i: (i, 0))

    sems = pltpu.SemaphoreType.DMA
    return pl.pallas_call(
        functools.partial(fused_kernel, tp, sp),
        grid=(nb,),
        in_specs=[rows(feats), whole(1, feats)] + [whole(feats, width)] * 4
        + [whole(feats, channels)] * 3
        + [whole(1, width), rows(width), whole(1, GROUP_FEATURES), whole(TAPS, channels),
           whole(1, GROUP_FEATURES)]
        + [pl.BlockSpec(memory_space=pl.ANY)] * 2,
        out_specs=whole(count, ncols),
        out_shape=jax.ShapeDtypeStruct((count, ncols), bf16),
        scratch_shapes=[
            pltpu.VMEM((HALO + ROWS, channels), f32),
            pltpu.VMEM((heads, GROUP_FEATURES, GROUP_FEATURES), f32),
            pltpu.VMEM((HALO, width), f32),
            pltpu.VMEM((count, width), f32),
            pltpu.VMEM((count, width), bf16),
            pltpu.VMEM((count, width), bf16),
            pltpu.VMEM((tp, nb, ROWS, channels), bf16),
            pltpu.VMEM((tp, nb, ROWS, width), bf16),
            pltpu.VMEM((2, tp, width, ncols), bf16),
            pltpu.VMEM((sp, heads, GROUP_FEATURES, GROUP_FEATURES), bf16),
            pltpu.VMEM((sp, HALO, width), f32),
            pltpu.VMEM((heads, GROUP_FEATURES, GROUP_FEATURES), bf16),
            pltpu.VMEM((HALO, channels), f32),
            pltpu.VMEM((HALO, channels), f32),
            pltpu.VMEM((HALO, channels), f32),
            pltpu.VMEM((HALO, channels), f32),
            pltpu.VMEM((heads, GROUP_FEATURES, GROUP_FEATURES), f32),
            sems((2, tp)), sems((2, tp)), sems((2,)),
            sems((2, tp // 2, nb)), sems((2, tp // 2, nb)), sems((2, tp, nb)),
            sems((sp,)), sems((sp,)), sems((sp,)), sems((sp,)), sems((1,)), sems((1,)),
        ],
        compiler_params=pltpu.CompilerParams(
            vmem_limit_bytes=56 * 2**20, collective_id=0, has_side_effects=True
        ),
    )(
        tokens, in_gain[None], w_query, w_forget, w_input, w_outgate, w_conv_h, w_conv_b, w_conv_c,
        forget_floor[None], forget_leak, state_gain[None], conv_taps, group_gain[None],
        out_state, out_conv,
    )


def solution(mesh):
    cols, rows = P(None, "tp"), P("tp", None)
    in_specs = (
        P("sp", None), P(), cols, cols, cols, cols, cols, cols, cols,
        P("tp"), P("sp", "tp"), P(), cols, P(), rows, rows,
    )
    return jax.shard_map(
        body, mesh=mesh, in_specs=in_specs, out_specs=P("sp", "tp"), check_vma=False
    )
```

time: 158 us -> 63.1 us (0.40)
  blocking collectives: 101 us -> 0 us
  Pallas kernels: 21.9 us -> 60.7 us
  between operations: 13.5 us -> 0.01 us
  local copies, waits for them, and re-layouts: 10.5 us -> 2.26 us
  matrix products: 6.16 us -> 0 us
  starting transfers between devices: 4.87 us -> 0 us
    all_to_all x1 -> x0, blocking collectives: 50.7 us -> none  [body(): lax.all_to_all(weight_rows, 'tp', split_axis=1, concat_axis=0, tiled=True)]
    all_gather x2 -> x0, blocking collectives: 50.1 us -> none  [the longest x1 31.9 us: body(): states = lax.all_gather(state, 'sp')]
    pallas_call x2 -> x1, Pallas kernels: 21.9 us -> 60.7 us  [body(): pl.pallas_call(functools.partial(fused_kernel, tp, sp), grid=(nb,), in_sp...]
    dot_general x1 -> x0, matrix products: 6.16 us -> none  [body(): return jnp.dot(everything, columns, preferred_element_type=f32).astype(bf16)]
    unnamed x22 -> x1, local copies, waits for them, and re-layouts: 8.09 us -> 2.26 us
    ppermute x1 -> x0, starting transfers between devices: 4.87 us -> none  [body(): rim = lax.ppermute(tail, 'sp', [(i, i + 1) for i in range(size - 1)])]
    all_to_all x1 -> x0, local copies, waits for them, and re-layouts: 2.38 us -> none  [body(): lax.all_to_all(weight_rows, 'tp', split_axis=1, concat_axis=0, tiled=True)]
  transfers between devices with their start and end apart: 2 -> 0, of which waited for: 0 -> 0; matrix products, arithmetic and copies ran while one was open for 2% -> 0% of each run, Pallas kernels for 0% -> 0%
where the time goes in v2:
time: 63.1 us; the launch traced here: 62.9 us
  Pallas kernels  60.7 us (96%)
  local copies, waits for them, and re-layouts  2.26 us (4%)
    pallas_call x1, Pallas kernels, body(): pl.pallas_call(functools.partial(fused_kernel, tp, sp), grid=(nb,), in_sp...  60.7 us
    unnamed x1, local copies, waits for them, and re-layouts  2.26 us

profile of v2, /device:TPU:0, one launch (start us, length us, event | category | flops | bytes accessed | tf_op | source)
XLA Modules:
  0.0 62.9 jit_solution(18409838214980542585)
XLA Ops:
  0.0 60.7 %shard_map.154 = bf16[1024,512]{1,0:T(8,128)(2,1)} custom-call(bf16[1024,2048]{1,0:T(8,128)(2,1)} %tokens.1, f32[1,2048]{1,0:T(1,128)} %bitcast.4, bf16[2048,256]{1,0:T(8,128)(2,1)} %wq.1, bf16[2048,256]{1,0:T(8,128)(2,1)} %wf.1, bf16[2048,256]{1,0:T(8,128)(2,1)} %wi.1, bf16[2048,256]{1,0:T(8,128)(2,1)} %wg.1, bf16[2048,256]{1,0:T(8,128)(2,1)} %wh.1, ...), custom_call_target="tpu_custom_call" | custom-call | tf_op jit(solution)/shard_map/pallas_call | solution.py:301
  60.7 2.3 %copy.18 = bf16[1024,512]{1,0:T(8,128)(2,1)} copy(bf16[1024,512]{1,0:T(8,128)(2,1)} %shard_map.154) | data formatting | bytes 2097152
